TPU v7x, 32 devices: a whole 2x2x4 slice. The times are simulated.
32 devices in a mesh: sp: 8 (over z, core), tp: 4 (over y, x).
Axes of the slice: x: 2, y: 2, z: 4, core: 2. Of those that a mesh axis runs over, the one named last changes fastest.
Arguments:
- query_a: bfloat16 [1024, 1024], P('tp', 'sp'), may hold values from -16 to 16
- key_a: bfloat16 [1024, 1024], P('tp', 'sp'), may hold values from -6 to 6
- value_a: bfloat16 [1024, 1024], P('tp', 'sp'), may hold values from -6 to 6
- cumlog_a: float32 [16, 1024], P('tp'), as said below
- query_b: bfloat16 [2048, 1024], P('tp', 'sp'), may hold values from -16 to 16
- key_b: bfloat16 [2048, 1024], P('tp', 'sp'), may hold values from -6 to 6
- value_b: bfloat16 [2048, 1024], P('tp', 'sp'), may hold values from -6 to 6
- cumlog_b: float32 [16, 1024], P('tp'), as said below
- out_weight_a: bfloat16 [1024, 2048], P('tp'), may hold values from -0.375 to 0.375
- out_weight_b: bfloat16 [2048, 2048], P('tp'), may hold values from -0.25 to 0.25
- residual: bfloat16 [1024, 2048], P(('sp', 'tp')), may hold values from -6 to 6
- norm_gain: float32 [2048], replicated, may hold values from 0.1 to 1.9
- expert_ids: int32 [1024, 2], P('sp'), may hold values from 0 to 7, as said below
- route_weight: float32 [1024, 2], P('sp'), may hold values from 0.1 to 1
- gate_w: bfloat16 [8, 2048, 1024], P('sp', None, 'tp'), may hold values from -0.125 to 0.125
- up_w: bfloat16 [8, 2048, 1024], P('sp', None, 'tp'), may hold values from -0.125 to 0.125
- down_w: bfloat16 [8, 1024, 2048], P('sp', None, 'tp'), may hold values from -0.1875 to 0.1875
Outputs:
- layer_out: bfloat16 [1024, 2048], P('sp', 'tp')
Inputs may be any that keep to these rules, and one draw needn't show every extreme that they name: `expert_ids`: each row names two different experts of one group (expert e is in group e // 2). In every aligned block of 128 rows (one index of sp) no expert is named more than 64 times, and every expert of one group, the same group for all blocks, is named exactly 64 times. `cumlog_a`: along positions the values of each head never increase. `cumlog_b`: along positions the values of each head never increase.
All inputs are finite; a program needn't handle non-finite values.
Results may differ from a plain program's by a relative error of at most 0.017.
Values may be sent and summed in bfloat16 or wider, within the bound.
A program may use at most 64 MiB of HBM per device.

v0:
```python
import jax
import jax.numpy as jnp
from jax import lax
from jax.sharding import PartitionSpec as P

HDA = 64
HDB = 128
GROUPS = 4
TOP = 2
norm_eps = 1e-05


def fold_group(state, queries, keys_piece, values_piece, cum_query, cum_key, visible, head_size):
    best, total, accum = state
    heads = best.shape[0]
    count = keys_piece.shape[1]
    key_grid = keys_piece.reshape(heads, head_size, count)
    value_grid = values_piece.reshape(heads, head_size, count)
    scores = jnp.einsum(
        "hdq,hdk->hqk", queries, key_grid, preferred_element_type=jnp.float32
    ) * head_size ** (-0.5)
    scores = scores + cum_query[:, :, None] - cum_key[:, None, :]
    scores = jnp.where(visible, scores, -jnp.inf)
    best_new = jnp.max(scores, axis=-1)
    shift = jnp.where(best_new > -jnp.inf, best_new, 0.0)
    keep_old = jnp.exp(best - shift)
    weights = jnp.exp(scores - shift[:, :, None])
    total_new = total * keep_old + jnp.sum(weights, axis=-1)
    added = jnp.einsum(
        "hqk,hdk->hdq", weights.astype(jnp.bfloat16), value_grid, preferred_element_type=jnp.float32
    )
    return (best_new, total_new, accum * keep_old[:, None, :] + added)


def empty_state(heads, head_size, length):
    return (
        jnp.full((heads, length), -jnp.inf, jnp.float32),
        jnp.zeros((heads, length), jnp.float32),
        jnp.zeros((heads, head_size, length), jnp.float32),
    )


def finish_state(state):
    accum = state[2] / state[1][:, None, :]
    return accum.astype(jnp.bfloat16).reshape(-1, accum.shape[2])


def per_device(
    query_a,
    key_a,
    value_a,
    cumlog_a,
    query_b,
    key_b,
    value_b,
    cumlog_b,
    out_weight_a,
    out_weight_b,
    residual,
    norm_gain,
    expert_ids,
    route_weight,
    gate_w,
    up_w,
    down_w,
):
    local_tokens = query_a.shape[1]
    heads_a = cumlog_a.shape[0]
    heads_b = cumlog_b.shape[0]
    my_start = lax.axis_index("sp") * local_tokens
    last_query = my_start + local_tokens - 1
    query_pos = my_start + jnp.arange(local_tokens, dtype=jnp.int32)
    cum_query_a = lax.dynamic_slice_in_dim(cumlog_a, my_start, local_tokens, 1)
    cum_query_b = lax.dynamic_slice_in_dim(cumlog_b, my_start, local_tokens, 1)
    grid_a = query_a.reshape(heads_a, HDA, local_tokens)
    grid_b = query_b.reshape(heads_b, HDB, local_tokens)
    keys_a = lax.all_gather(key_a, "sp", axis=1, tiled=True)
    vals_a = lax.all_gather(value_a, "sp", axis=1, tiled=True)
    keys_b = lax.all_gather(key_b, "sp", axis=1, tiled=True)
    vals_b = lax.all_gather(value_b, "sp", axis=1, tiled=True)
    count = keys_a.shape[1]

    def visit(state):
        key_pos = jnp.arange(count, dtype=jnp.int32)
        visible = key_pos[None, None, :] <= query_pos[None, :, None]
        new_a = fold_group(state[0], grid_a, keys_a, vals_a, cum_query_a, cumlog_a, visible, HDA)
        new_b = fold_group(state[1], grid_b, keys_b, vals_b, cum_query_b, cumlog_b, visible, HDB)
        return (new_a, new_b)

    def leave(state):
        return state

    state_a, state_b = lax.cond(
        jnp.int32(0) <= last_query,
        visit,
        leave,
        (empty_state(heads_a, HDA, local_tokens), empty_state(heads_b, HDB, local_tokens)),
    )
    attn_a = finish_state(state_a)
    attn_b = finish_state(state_b)
    term = lax.dot_general(
        attn_a, out_weight_a, (((0,), (0,)), ((), ())), preferred_element_type=jnp.float32
    )
    mixed = lax.psum_scatter(
        (
            term
            + lax.dot_general(
                attn_b, out_weight_b, (((0,), (0,)), ((), ())), preferred_element_type=jnp.float32
            )
        ).astype(jnp.bfloat16),
        "tp",
        scatter_dimension=0,
        tiled=True,
    ).astype(jnp.float32)
    summed = residual.astype(jnp.float32) + mixed
    center = summed - jnp.mean(summed, axis=-1, keepdims=True)
    variance = jnp.mean(center * center, axis=-1, keepdims=True)
    normed = (center * lax.rsqrt(variance + norm_eps) * norm_gain).astype(jnp.bfloat16)
    normed_all = lax.all_gather(normed, "tp", axis=0, tiled=True)
    experts = lax.axis_size("sp")
    group_size = experts // GROUPS
    capacity = local_tokens // group_size
    features = normed_all.shape[1]
    flat_ids = expert_ids.reshape(-1)
    marks = (flat_ids[:, None] == jnp.arange(experts, dtype=jnp.int32)[None, :]).astype(jnp.int32)
    rank = jnp.sum((jnp.cumsum(marks, axis=0) - marks) * marks, axis=1)
    slot = flat_ids * capacity + rank
    token_of = jnp.arange(local_tokens * TOP, dtype=jnp.int32) // TOP
    table = jnp.zeros((experts * capacity,), jnp.int32).at[slot].set(token_of)
    filled = jnp.zeros((experts * capacity,), jnp.bfloat16).at[slot].set(1.0)
    send = (normed_all[table] * filled[:, None]).reshape(experts, capacity, features)
    rows = lax.all_to_all(send, "sp", split_axis=0, concat_axis=0, tiled=True)
    sources, items, row_width = rows.shape
    flat_rows = rows.reshape(sources * items, row_width)
    gate = jnp.dot(flat_rows, gate_w[0], preferred_element_type=jnp.float32)
    upper = jnp.dot(flat_rows, up_w[0], preferred_element_type=jnp.float32)
    hidden = (jax.nn.silu(gate) * upper).astype(jnp.bfloat16).reshape(sources, items, -1)
    hidden_all = lax.all_gather(hidden, "tp", axis=2, tiled=True)
    result = jnp.dot(
        hidden_all.reshape(sources * items, -1), down_w[0], preferred_element_type=jnp.float32
    )
    result = result.astype(jnp.bfloat16).reshape(sources, items, -1)
    returned = lax.all_to_all(result, "sp", split_axis=0, concat_axis=0, tiled=True)
    flat_back = returned.reshape(experts * capacity, -1)
    picked = flat_back[slot].reshape(local_tokens, TOP, -1).astype(jnp.float32)
    routed = jnp.sum(picked * route_weight[:, :, None], axis=1)
    columns = routed.shape[1]
    own_cols = lax.dynamic_slice_in_dim(normed_all, lax.axis_index("tp") * columns, columns, 1)
    return (own_cols.astype(jnp.float32) + routed).astype(jnp.bfloat16)


def solution(mesh):
    placed = (
        P("tp", "sp"),
        P("tp", "sp"),
        P("tp", "sp"),
        P("tp", None),
        P("tp", "sp"),
        P("tp", "sp"),
        P("tp", "sp"),
        P("tp", None),
        P("tp", None),
        P("tp", None),
        P(("sp", "tp"), None),
        P(),
        P("sp", None),
        P("sp", None),
        P("sp", None, "tp"),
        P("sp", None, "tp"),
        P("sp", None, "tp"),
    )
    return jax.shard_map(
        per_device, mesh=mesh, in_specs=placed, out_specs=P("sp", "tp"), check_vma=False
    )
```

profile of v0, /device:TPU:0, one launch (start us, length us, event | category | flops | bytes accessed | tf_op | source)
XLA Modules:
  0.0 229.1 jit_solution(7319173430591822474)
XLA Ops:
  6.5 0.7 all-gather.4.cloned.1.call-update
  8.1 0.8 copy.27
  9.0 0.7 eq.25
  10.6 17.6 %all_gather.18 = bf16[256,1024]{1,0:T(8,128)(2,1)S(1)} all-gather(bf16[256,128]{1,0:T(8,128)(2,1)} %param.20), channel_id=1, replica_groups=mesh['sp'=8,'tp'=4] {'sp'}, dimensions={1}, use_global_device_ids=true | all-gather | bytes 589824 | tf_op jit(solution)/shard_map/all_gather | solution.py:77
  28.2 14.7 %all_gather.19 = bf16[256,1024]{1,0:T(8,128)(2,1)S(1)} all-gather(bf16[256,128]{1,0:T(8,128)(2,1)} %param.21), channel_id=1, replica_groups=mesh['sp'=8,'tp'=4] {'sp'}, dimensions={1}, use_global_device_ids=true | all-gather | bytes 589824 | tf_op jit(solution)/shard_map/all_gather | solution.py:78
  42.9 19.9 %all-gather.6.cloned.1.call-done = bf16[512,1024]{1,0:T(8,128)(2,1)} async-done(((bf16[512,128]{1,0:T(8,128)(2,1)}), bf16[512,1024]{1,0:T(8,128)(2,1)}) %all-gather.6.cloned.1.call-update) | async-done | bytes 1048592 | tf_op jit(solution)/shard_map/all_gather | solution.py:80
  62.8 7.6 %conditional.1 = (f32[4,128]{1,0:T(4,128)S(1)}, f32[4,64,128]{2,1,0:T(8,128)S(1)}, f32[4,128]{1,0:T(4,128)S(1)}, f32[4,128,128]{2,1,0:T(8,128)S(1)}) conditional(s32[]{:T(128)} %convert_element_type.59, () %tuple.20, (s32[]{:T(128)}, s32[128]{0:T(128)S(1)}, bf16[256,128]{1,0:T(8,128)(2,1)}, bf16[256,1024]{1,0:T(8,128)(2,1)S(1)}, f32[4,1024]{1,0:T(4,128)}, ...), branch_computations={%region_0.0_spmd, %region_1.6_spmd} | conditional | flops 412324992 | bytes 26306234 | solution.py:93
  62.8 0.8 constant_dynamic-slice_fusion
  63.7 1.6 fusion.27
  66.6 0.8 fusion.28
  68.0 1.3 fusion.4
  69.3 1.1 copy.32
  70.4 1.6 fusion.29
  72.1 1.3 fusion.12
  74.4 1.4 scatter_custom_fusion
  75.8 2.2 scatter_custom_fusion.1
  78.0 19.3 %reduce-scatter.2.cloned.1.call-done = bf16[32,2048]{1,0:T(8,128)(2,1)} async-done(((bf16[128,2048]{1,0:T(8,128)(2,1)}), bf16[32,2048]{1,0:T(8,128)(2,1)}) %reduce-scatter.2.cloned.1.call-update) | async-done | bytes 131088 | tf_op jit(solution)/shard_map/reduce_scatter | solution.py:104
  97.3 1.0 fusion.19
  98.4 1.1 multiply_reduce_fusion.1
  99.5 1.0 multiply_convert_fusion
  100.5 10.2 %all_gather.22 = bf16[128,2048]{1,0:T(8,128)(2,1)S(1)} all-gather(bf16[32,2048]{1,0:T(8,128)(2,1)S(1)} %multiply_convert_fusion), channel_id=1, replica_groups=mesh['sp'=8,'tp'=4] {'tp'}, dimensions={0}, use_global_device_ids=true | all-gather | bytes 655360 | tf_op jit(solution)/shard_map/all_gather | solution.py:119
  110.8 3.3 %gather_fusion = bf16[512,2048]{1,0:T(8,128)(2,1)} fusion(bf16[128,2048]{1,0:T(8,128)(2,1)S(1)} %all_gather.22, s32[1024]{0:T(1024)S(1)} %pad_clamp_fusion.1), kind=kCustom, calls=%fused_computation | custom fusion | bytes 4196352 | tf_op jit(solution)/shard_map/gather | solution.py:131
  114.1 1.8 broadcast_multiply_fusion
  115.9 53.6 %all_to_all.10 = bf16[8,64,2048]{2,1,0:T(8,128)(2,1)S(1)} all-to-all(bf16[8,64,2048]{2,1,0:T(8,128)(2,1)S(1)} %broadcast_multiply_fusion), channel_id=1, replica_groups=mesh['sp'=8,'tp'=4] {'sp'}, dimensions={0} | all-to-all | bytes 4194304 | tf_op jit(solution)/shard_map/all_to_all | solution.py:132
  169.5 0.7 fusion.16
  170.8 1.4 fusion.13
  172.2 24.5 %all-gather.8.cloned.1.call-done = bf16[8,64,1024]{2,1,0:T(8,128)(2,1)} async-done(((bf16[8,64,256]{2,1,0:T(8,128)(2,1)}), bf16[8,64,1024]{2,1,0:T(8,128)(2,1)}) %all-gather.8.cloned.1.call-update) | async-done | bytes 1048592 | tf_op jit(solution)/shard_map/all_gather | solution.py:138
  196.7 3.1 %convolution_convert_fusion = bf16[512,512]{1,0:T(8,128)(2,1)} fusion(bf16[512,1024]{1,0:T(8,128)(2,1)} %bitcast.66, bf16[1,1024,512]{2,1,0:T(8,128)(2,1)} %param.35), kind=kOutput, calls=%fused_computation.30 | convolution fusion | flops 537133056 | bytes 2621440 | tf_op jit(solution)/shard_map/dot_general | solution.py:139
  199.8 4.6 %all-to-all-start.1 = ((bf16[8,64,512]{2,1,0:T(8,128)(2,1)}), bf16[8,64,512]{2,1,0:T(8,128)(2,1)S(1)}, u32[]{:S(2)}, u32[]{:S(2)}) async-start(bf16[8,64,512]{2,1,0:T(8,128)(2,1)} %bitcast.57), calls=%async_computation.2 | async-start | bytes 1048576 | tf_op jit(solution)/shard_map/all_to_all | solution.py:143
  204.5 15.2 %all-to-all-done.1 = bf16[8,64,512]{2,1,0:T(8,128)(2,1)S(1)} async-done(((bf16[8,64,512]{2,1,0:T(8,128)(2,1)}), bf16[8,64,512]{2,1,0:T(8,128)(2,1)S(1)}, u32[]{:S(2)}, u32[]{:S(2)}) %all-to-all-start.1) | async-done | bytes 524320 | tf_op jit(solution)/shard_map/all_to_all | solution.py:143
  219.7 1.2 gather_fusion.1
  221.2 0.7 multiply_reduce_fusion
  (64 shorter events, 6.6 us)
Async XLA Ops:
  6.5 65.5 %copy-start = (bf16[512,2048]{1,0:T(8,128)(2,1)S(1)}, bf16[512,2048]{1,0:T(8,128)(2,1)}, u32[]{:S(2)}) copy-start(bf16[512,2048]{1,0:T(8,128)(2,1)} %param.28) | copy-start | bytes 6291460
  6.5 36.4 %all-gather.4.cloned.1.call-start = ((), (), s32[]{:S(2)}) async-start(), calls=%async_computation.3 | async-start | bytes 1179648 | tf_op jit(solution)/shard_map/all_gather | solution.py:79
  7.3 55.5 %all-gather.6.cloned.1.call-start = ((), (), s32[]{:S(2)}) async-start(), calls=%async_computation.4 | async-start | bytes 1179648 | tf_op jit(solution)/shard_map/all_gather | solution.py:80
  8.0 89.3 %reduce-scatter.2.cloned.1.call-start = ((), (), s32[]{:S(2)}) async-start(), calls=%async_computation.5 | async-start | bytes 655360 | tf_op jit(solution)/shard_map/reduce_scatter | solution.py:104
  65.4 1.2 copy-start.6
  65.4 1.2 copy-start.9
  65.4 1.2 copy-start.10
  66.6 1.4 copy-start.2
  72.0 2.2 copy-start.4
  72.0 25.3 %copy-start.1 = (bf16[32,2048]{1,0:T(8,128)(2,1)S(1)}, bf16[32,2048]{1,0:T(8,128)(2,1)}, u32[]{:S(2)}) copy-start(bf16[32,2048]{1,0:T(8,128)(2,1)} %param.29) | copy-start | bytes 393220
  72.0 27.5 %copy-start.3 = (f32[2048]{0:T(1024)S(1)}, f32[2048]{0:T(1024)}, u32[]{:S(2)}) copy-start(f32[2048]{0:T(1024)} %param.30) | copy-start | bytes 24580
  73.3 123.4 %all-gather.8.cloned.1.call-start = ((), (), s32[]{:S(2)}) async-start(), calls=%async_computation.6 | async-start | bytes 1310720 | tf_op jit(solution)/shard_map/all_gather | solution.py:138
  115.9 53.6 %copy-start.7 = (bf16[1,2048,256]{2,1,0:T(8,128)(2,1)S(1)}, bf16[1,2048,256]{2,1,0:T(8,128)(2,1)}, u32[]{:S(2)}) copy-start(bf16[1,2048,256]{2,1,0:T(8,128)(2,1)} %param.33) | copy-start | bytes 3145732
  169.5 1.2 copy-start.8
  196.7 7.7 %copy-start.5 = (f32[128,2]{0,1:T(2,128)S(1)}, f32[128,2]{0,1:T(2,128)}, u32[]{:S(2)}) copy-start(f32[128,2]{0,1:T(2,128)} %param.32) | copy-start | bytes 3076
  199.8 19.9 %all-to-all-start.1 = ((bf16[8,64,512]{2,1,0:T(8,128)(2,1)}), bf16[8,64,512]{2,1,0:T(8,128)(2,1)S(1)}, u32[]{:S(2)}, u32[]{:S(2)}) async-start(bf16[8,64,512]{2,1,0:T(8,128)(2,1)} %bitcast.57), calls=%async_computation.2 | async-start | bytes 1048576 | tf_op jit(solution)/shard_map/all_to_all | solution.py:143
Sparse Core Ops, SparseCore 0:
  8.9 27.7 all-gather.3
  38.3 24.4 all-gather.5
  73.5 23.8 reduce-scatter.1
  172.3 24.3 all-gather.7
where the time goes:
time: 230 us; the launch traced here: 229 us
  blocking collectives  96.1 us (42%)
  waiting for transfers between devices  80.3 us (35%)
  between operations  13.3 us (6%)
  local copies, waits for them, and re-layouts  13.2 us (6%)
  matrix products  12.4 us (5%)
  other arithmetic  9.06 us (4%)
  starting transfers between devices  4.73 us (2%)
    all_to_all x1, blocking collectives, per_device(): rows = lax.all_to_all(send, 'sp', split_axis=0, concat_axis=0, tiled=True)  53.6 us
    all_gather x1, waiting for transfers between devices, per_device(): hidden_all = lax.all_gather(hidden, 'tp', axis=2, tiled=True)  24.5 us
    all_gather x1, waiting for transfers between devices, per_device(): vals_b = lax.all_gather(value_b, 'sp', axis=1, tiled=True)  19.9 us
    reduce_scatter x1, waiting for transfers between devices, per_device(): lax.psum_scatter((term + lax.dot_general(attn_b, out_weight_b, (((0,), (0...  19.3 us
    all_gather x1, blocking collectives, per_device(): keys_a = lax.all_gather(key_a, 'sp', axis=1, tiled=True)  17.6 us
    all_to_all x1, waiting for transfers between devices, per_device(): lax.all_to_all(result, 'sp', split_axis=0, concat_axis=0, tiled=True)  15.2 us
    all_gather x1, blocking collectives, per_device(): vals_a = lax.all_gather(value_a, 'sp', axis=1, tiled=True)  14.7 us
    all_gather x1, blocking collectives, per_device(): normed_all = lax.all_gather(normed, 'tp', axis=0, tiled=True)  10.2 us
  transfers between devices with their start and end apart: 5, of which 4 were waited for; matrix products, arithmetic and copies ran while one was open for 3% of the time, Pallas kernels for 0%

commit v1 on v0

--- a/solution.py
+++ b/solution.py
@@ -75,7 +75,12 @@
     grid_a = query_a.reshape(heads_a, HDA, local_tokens)
     grid_b = query_b.reshape(heads_b, HDB, local_tokens)
     keys_a = lax.all_gather(key_a, "sp", axis=1, tiled=True)
-    vals_a = lax.all_gather(value_a, "sp", axis=1, tiled=True)
+    ring = [value_a]
+    for hop in range(7):
+        ring.append(lax.ppermute(ring[-1], "sp", [(dev, (dev + 1) % 8) for dev in range(8)]))
+    vals_a = jnp.roll(
+        jnp.concatenate(ring[::-1], axis=1), (lax.axis_index("sp") + 1) * ring[0].shape[1], axis=1
+    )
     keys_b = lax.all_gather(key_b, "sp", axis=1, tiled=True)
     vals_b = lax.all_gather(value_b, "sp", axis=1, tiled=True)
     count = keys_a.shape[1]

time: 230 us -> 237 us (1.030)
  blocking collectives: 96.1 us -> 80.4 us
  waiting for transfers between devices: 80.3 us -> 92.7 us
  local copies, waits for them, and re-layouts: 13.2 us -> 20.5 us
    ppermute x0 -> x7, waiting for transfers between devices: none -> 33.6 us  [per_device(): lax.ppermute(ring[-1], 'sp', [(dev, (dev + 1) % 8) for dev in range(8)])]
    all_gather x1, waiting for transfers between devices: 19.9 us -> 0.02 us  [per_device(): vals_b = lax.all_gather(value_b, 'sp', axis=1, tiled=True)]
    all_gather x1 -> x0, blocking collectives: 14.7 us -> none  [per_device(): vals_a = lax.all_gather(value_a, 'sp', axis=1, tiled=True)]
    unnamed x16 -> x39, local copies, waits for them, and re-layouts: 1.44 us -> 5.41 us
  transfers between devices with their start and end apart: 5 -> 12, of which waited for: 4 -> 9; matrix products, arithmetic and copies ran while one was open for 3% -> 5% of each run, Pallas kernels for 0% -> 0%
where the time goes in v1:
time: 237 us; the launch traced here: 236 us
  waiting for transfers between devices  92.7 us (39%)
  blocking collectives  80.4 us (34%)
  local copies, waits for them, and re-layouts  20.5 us (9%)
  matrix products  13.8 us (6%)
  between operations  13.4 us (6%)
  other arithmetic  9.71 us (4%)
  starting transfers between devices  5.67 us (2%)
    all_to_all x1, blocking collectives, per_device(): rows = lax.all_to_all(send, 'sp', split_axis=0, concat_axis=0, tiled=True)  53.6 us
    ppermute x7, waiting for transfers between devices, per_device(): lax.ppermute(ring[-1], 'sp', [(dev, (dev + 1) % 8) for dev in range(8)])  33.6 us
    all_gather x1, waiting for transfers between devices, per_device(): hidden_all = lax.all_gather(hidden, 'tp', axis=2, tiled=True)  24.5 us
    reduce_scatter x1, waiting for transfers between devices, per_device(): lax.psum_scatter((term + lax.dot_general(attn_b, out_weight_b, (((0,), (0...  18.7 us
    all_gather x1, blocking collectives, per_device(): keys_a = lax.all_gather(key_a, 'sp', axis=1, tiled=True)  16.5 us
    all_to_all x1, waiting for transfers between devices, per_device(): lax.all_to_all(result, 'sp', split_axis=0, concat_axis=0, tiled=True)  15.2 us
    all_gather x1, blocking collectives, per_device(): normed_all = lax.all_gather(normed, 'tp', axis=0, tiled=True)  10.3 us
    unnamed x39, local copies, waits for them, and re-layouts  5.41 us
  transfers between devices with their start and end apart: 12, of which 9 were waited for; matrix products, arithmetic and copies ran while one was open for 5% of the time, Pallas kernels for 0%

profile of v1, /device:TPU:0, one launch (start us, length us, event | category | flops | bytes accessed | tf_op | source)
XLA Modules:
  0.0 236.3 jit_solution(11625262327277251841)
XLA Ops:
  7.9 6.2 %collective-permute-done = bf16[256,128]{1,0:T(8,128)(2,1)S(1)} collective-permute-done((bf16[256,128]{1,0:T(8,128)(2,1)}, bf16[256,128]{1,0:T(8,128)(2,1)S(1)}, u32[]{:S(2)}, u32[]{:S(2)}) %collective-permute-start) | collective-permute-done | bytes 65568 | tf_op jit(solution)/shard_map/ppermute | solution.py:80
  14.0 5.5 %collective-permute-done.1 = bf16[256,128]{1,0:T(8,128)(2,1)S(1)} collective-permute-done((bf16[256,128]{1,0:T(8,128)(2,1)S(1)}, bf16[256,128]{1,0:T(8,128)(2,1)S(1)}, u32[]{:S(2)}, u32[]{:S(2)}) %collective-permute-start.1) | collective-permute-done | bytes 65568 | tf_op jit(solution)/shard_map/ppermute | solution.py:80
  19.5 6.7 %collective-permute-done.2 = bf16[256,128]{1,0:T(8,128)(2,1)S(1)} collective-permute-done((bf16[256,128]{1,0:T(8,128)(2,1)S(1)}, bf16[256,128]{1,0:T(8,128)(2,1)S(1)}, u32[]{:S(2)}, u32[]{:S(2)}) %collective-permute-start.2) | collective-permute-done | bytes 65568 | tf_op jit(solution)/shard_map/ppermute | solution.py:80
  26.3 6.6 %collective-permute-done.3 = bf16[256,128]{1,0:T(8,128)(2,1)S(1)} collective-permute-done((bf16[256,128]{1,0:T(8,128)(2,1)S(1)}, bf16[256,128]{1,0:T(8,128)(2,1)S(1)}, u32[]{:S(2)}, u32[]{:S(2)}) %collective-permute-start.3) | collective-permute-done | bytes 65568 | tf_op jit(solution)/shard_map/ppermute | solution.py:80
  33.0 5.4 %collective-permute-done.4 = bf16[256,128]{1,0:T(8,128)(2,1)S(1)} collective-permute-done((bf16[256,128]{1,0:T(8,128)(2,1)S(1)}, bf16[256,128]{1,0:T(8,128)(2,1)S(1)}, u32[]{:S(2)}, u32[]{:S(2)}) %collective-permute-start.4) | collective-permute-done | bytes 65568 | tf_op jit(solution)/shard_map/ppermute | solution.py:80
  38.4 16.5 %all_gather.15 = bf16[256,1024]{1,0:T(8,128)(2,1)} all-gather(bf16[256,128]{1,0:T(8,128)(2,1)} %param.20), channel_id=1, replica_groups=mesh['sp'=8,'tp'=4] {'sp'}, dimensions={1}, use_global_device_ids=true | all-gather | bytes 589824 | tf_op jit(solution)/shard_map/all_gather | solution.py:77
  57.9 3.1 %collective-permute-done.6 = bf16[256,128]{1,0:T(8,128)(2,1)} collective-permute-done((bf16[256,128]{1,0:T(8,128)(2,1)S(1)}, bf16[256,128]{1,0:T(8,128)(2,1)}, u32[]{:S(2)}, u32[]{:S(2)}) %collective-permute-start.6) | collective-permute-done | bytes 65568 | tf_op jit(solution)/shard_map/ppermute | solution.py:80
  65.8 13.7 %conditional.1 = (f32[4,128]{1,0:T(4,128)S(1)}, f32[4,64,128]{2,1,0:T(8,128)S(1)}, f32[4,128]{1,0:T(4,128)S(1)}, f32[4,128,128]{2,1,0:T(8,128)S(1)}) conditional(s32[]{:T(128)} %convert_element_type.61, () %tuple.26, (s32[]{:T(128)}, s32[128]{0:T(128)}, bf16[256,128]{1,0:T(8,128)(2,1)}, bf16[256,1024]{1,0:T(8,128)(2,1)}, f32[4,1024]{1,0:T(4,128)}, ...), branch_computations={%region_0.1_spmd, %region_1.6_spmd.clone} | conditional | flops 412324992 | bytes 35219288 | solution.py:98
  67.4 1.8 fusion.26
  69.3 1.3 copy-done.1
  71.2 1.4 constant_dynamic-slice_fusion.1
  72.5 2.2 convolution_add_fusion.1
  74.7 1.8 fusion.27
  77.1 1.3 fusion.4
  78.4 1.1 copy.36
  79.9 1.3 fusion.11
  82.2 1.4 scatter_custom_fusion
  83.6 2.2 scatter_custom_fusion.1
  85.9 18.7 %reduce-scatter.2.cloned.1.call-done = bf16[32,2048]{1,0:T(8,128)(2,1)} async-done(((bf16[128,2048]{1,0:T(8,128)(2,1)}), bf16[32,2048]{1,0:T(8,128)(2,1)}) %reduce-scatter.2.cloned.1.call-update) | async-done | bytes 131088 | tf_op jit(solution)/shard_map/reduce_scatter | solution.py:109
  104.6 1.0 fusion.18
  105.6 1.1 multiply_reduce_fusion.1
  106.7 1.0 multiply_convert_fusion
  107.8 10.3 %all_gather.18 = bf16[128,2048]{1,0:T(8,128)(2,1)S(1)} all-gather(bf16[32,2048]{1,0:T(8,128)(2,1)S(1)} %multiply_convert_fusion), channel_id=1, replica_groups=mesh['sp'=8,'tp'=4] {'tp'}, dimensions={0}, use_global_device_ids=true | all-gather | bytes 655360 | tf_op jit(solution)/shard_map/all_gather | solution.py:124
  118.0 3.3 %gather_fusion = bf16[512,2048]{1,0:T(8,128)(2,1)} fusion(bf16[128,2048]{1,0:T(8,128)(2,1)S(1)} %all_gather.18, s32[1024]{0:T(1024)S(1)} %pad_clamp_fusion.1), kind=kCustom, calls=%fused_computation | custom fusion | bytes 4196352 | tf_op jit(solution)/shard_map/gather | solution.py:136
  121.4 1.8 broadcast_multiply_fusion
  123.2 53.6 %all_to_all.10 = bf16[8,64,2048]{2,1,0:T(8,128)(2,1)S(1)} all-to-all(bf16[8,64,2048]{2,1,0:T(8,128)(2,1)S(1)} %broadcast_multiply_fusion), channel_id=1, replica_groups=mesh['sp'=8,'tp'=4] {'sp'}, dimensions={0} | all-to-all | bytes 4194304 | tf_op jit(solution)/shard_map/all_to_all | solution.py:137
  178.0 1.4 fusion.12
  179.4 24.5 %all-gather.8.cloned.1.call-done = bf16[8,64,1024]{2,1,0:T(8,128)(2,1)} async-done(((bf16[8,64,256]{2,1,0:T(8,128)(2,1)}), bf16[8,64,1024]{2,1,0:T(8,128)(2,1)}) %all-gather.8.cloned.1.call-update) | async-done | bytes 1048592 | tf_op jit(solution)/shard_map/all_gather | solution.py:143
  203.9 3.1 %convolution_convert_fusion = bf16[512,512]{1,0:T(8,128)(2,1)} fusion(bf16[512,1024]{1,0:T(8,128)(2,1)} %bitcast.64, bf16[1,1024,512]{2,1,0:T(8,128)(2,1)} %param.35), kind=kOutput, calls=%fused_computation.30 | convolution fusion | flops 537133056 | bytes 2621440 | tf_op jit(solution)/shard_map/dot_general | solution.py:144
  207.0 4.6 %all-to-all-start.1 = ((bf16[8,64,512]{2,1,0:T(8,128)(2,1)}), bf16[8,64,512]{2,1,0:T(8,128)(2,1)S(1)}, u32[]{:S(2)}, u32[]{:S(2)}) async-start(bf16[8,64,512]{2,1,0:T(8,128)(2,1)} %bitcast.55), calls=%async_computation.2 | async-start | bytes 1048576 | tf_op jit(solution)/shard_map/all_to_all | solution.py:148
  211.7 15.2 %all-to-all-done.1 = bf16[8,64,512]{2,1,0:T(8,128)(2,1)S(1)} async-done(((bf16[8,64,512]{2,1,0:T(8,128)(2,1)}), bf16[8,64,512]{2,1,0:T(8,128)(2,1)S(1)}, u32[]{:S(2)}, u32[]{:S(2)}) %all-to-all-start.1) | async-done | bytes 524320 | tf_op jit(solution)/shard_map/all_to_all | solution.py:148
  226.9 1.2 gather_fusion.1
  (102 shorter events, 16.3 us)
Async XLA Ops:
  6.5 73.3 %copy-start = (bf16[512,2048]{1,0:T(8,128)(2,1)S(1)}, bf16[512,2048]{1,0:T(8,128)(2,1)}, u32[]{:S(2)}) copy-start(bf16[512,2048]{1,0:T(8,128)(2,1)} %param.28) | copy-start | bytes 6291460
  6.5 56.3 %copy-start.6 = (bf16[256,128]{1,0:T(8,128)(2,1)S(1)}, bf16[256,128]{1,0:T(8,128)(2,1)}, u32[]{:S(2)}) copy-start(bf16[256,128]{1,0:T(8,128)(2,1)} %param.21) | copy-start | bytes 196612
  6.5 58.3 %all-gather.4.cloned.1.call-start = ((), (), s32[]{:S(2)}) async-start(), calls=%async_computation.3 | async-start | bytes 1179648 | tf_op jit(solution)/shard_map/all_gather | solution.py:84
  7.3 57.6 %all-gather.6.cloned.1.call-start = ((), (), s32[]{:S(2)}) async-start(), calls=%async_computation.4 | async-start | bytes 1179648 | tf_op jit(solution)/shard_map/all_gather | solution.py:85
  7.3 6.7 %collective-permute-start = (bf16[256,128]{1,0:T(8,128)(2,1)}, bf16[256,128]{1,0:T(8,128)(2,1)S(1)}, u32[]{:S(2)}, u32[]{:S(2)}) collective-permute-start(bf16[256,128]{1,0:T(8,128)(2,1)} %param.21), channel_id=1, source_target_pairs={{0,4},{4,8},{8,12},{12,16},{16,20},{20,24},{24,28},{28,0},{1,5},{5... | collective-permute-start | bytes 196616 | tf_op jit(solution)/shard_map/ppermute | solution.py:80
  14.0 5.5 %collective-permute-start.1 = (bf16[256,128]{1,0:T(8,128)(2,1)S(1)}, bf16[256,128]{1,0:T(8,128)(2,1)S(1)}, u32[]{:S(2)}, u32[]{:S(2)}) collective-permute-start(bf16[256,128]{1,0:T(8,128)(2,1)S(1)} %collective-permute-done), channel_id=1, source_target_pairs={{0,4},{4,8},{8,12},{12,16},{16,20},{20,24},{24,28},{28,0},{1,5},{5... | collective-permute-start | bytes 196616 | tf_op jit(solution)/shard_map/ppermute | solution.py:80
  19.5 6.7 %collective-permute-start.2 = (bf16[256,128]{1,0:T(8,128)(2,1)S(1)}, bf16[256,128]{1,0:T(8,128)(2,1)S(1)}, u32[]{:S(2)}, u32[]{:S(2)}) collective-permute-start(bf16[256,128]{1,0:T(8,128)(2,1)S(1)} %collective-permute-done.1), channel_id=1, source_target_pairs={{0,4},{4,8},{8,12},{12,16},{16,20},{20,24},{24,28},{28,0},{1,5},{5... | collective-permute-start | bytes 196616 | tf_op jit(solution)/shard_map/ppermute | solution.py:80
  26.3 6.6 %collective-permute-start.3 = (bf16[256,128]{1,0:T(8,128)(2,1)S(1)}, bf16[256,128]{1,0:T(8,128)(2,1)S(1)}, u32[]{:S(2)}, u32[]{:S(2)}) collective-permute-start(bf16[256,128]{1,0:T(8,128)(2,1)S(1)} %collective-permute-done.2), channel_id=1, source_target_pairs={{0,4},{4,8},{8,12},{12,16},{16,20},{20,24},{24,28},{28,0},{1,5},{5... | collective-permute-start | bytes 196616 | tf_op jit(solution)/shard_map/ppermute | solution.py:80
  32.9 5.5 %collective-permute-start.4 = (bf16[256,128]{1,0:T(8,128)(2,1)S(1)}, bf16[256,128]{1,0:T(8,128)(2,1)S(1)}, u32[]{:S(2)}, u32[]{:S(2)}) collective-permute-start(bf16[256,128]{1,0:T(8,128)(2,1)S(1)} %collective-permute-done.3), channel_id=1, source_target_pairs={{0,4},{4,8},{8,12},{12,16},{16,20},{20,24},{24,28},{28,0},{1,5},{5... | collective-permute-start | bytes 196616 | tf_op jit(solution)/shard_map/ppermute | solution.py:80
  32.9 71.6 %reduce-scatter.2.cloned.1.call-start = ((), (), s32[]{:S(2)}) async-start(), calls=%async_computation.5 | async-start | bytes 655360 | tf_op jit(solution)/shard_map/reduce_scatter | solution.py:109
  38.4 16.5 %collective-permute-start.5 = (bf16[256,128]{1,0:T(8,128)(2,1)S(1)}, bf16[256,128]{1,0:T(8,128)(2,1)S(1)}, u32[]{:S(2)}, u32[]{:S(2)}) collective-permute-start(bf16[256,128]{1,0:T(8,128)(2,1)S(1)} %collective-permute-done.4), channel_id=1, source_target_pairs={{0,4},{4,8},{8,12},{12,16},{16,20},{20,24},{24,28},{28,0},{1,5},{5... | collective-permute-start | bytes 196616 | tf_op jit(solution)/shard_map/ppermute | solution.py:80
  54.9 3.0 %copy-start.7 = (bf16[256,128]{1,0:T(8,128)(2,1)}, bf16[256,128]{1,0:T(8,128)(2,1)S(1)}, u32[]{:S(2)}) copy-start(bf16[256,128]{1,0:T(8,128)(2,1)S(1)} %collective-permute-done.5) | copy-start | bytes 196612
  54.9 6.1 %collective-permute-start.6 = (bf16[256,128]{1,0:T(8,128)(2,1)S(1)}, bf16[256,128]{1,0:T(8,128)(2,1)}, u32[]{:S(2)}, u32[]{:S(2)}) collective-permute-start(bf16[256,128]{1,0:T(8,128)(2,1)S(1)} %collective-permute-done.5), channel_id=1, source_target_pairs={{0,4},{4,8},{8,12},{12,16},{16,20},{20,24},{24,28},{28,0},{1,5},{5... | collective-permute-start | bytes 196616 | tf_op jit(solution)/shard_map/ppermute | solution.py:80
  64.8 1.0 copy-start.5
  65.8 13.7 %copy-start.3 = (bf16[256,2048]{1,0:T(8,128)(2,1)S(1)}, bf16[256,2048]{1,0:T(8,128)(2,1)}, u32[]{:S(2)}) copy-start(bf16[256,2048]{1,0:T(8,128)(2,1)} %param.27) | copy-start | bytes 3145732
  69.2 1.3 copy-start.1
  71.1 3.6 %copy-start.11 = (f32[4,1024]{1,0:T(4,128)S(1)}, f32[4,1024]{1,0:T(4,128)}, u32[]{:S(2)}) copy-start(f32[4,1024]{1,0:T(4,128)} %get-tuple-element.275) | copy-start | bytes 49156 | tf_op jit(solution)/shard_map/cond
  71.1 3.6 %copy-start.14 = (bf16[512,1024]{1,0:T(8,128)(2,1)S(1)}, bf16[512,1024]{1,0:T(8,128)(2,1)}, u32[]{:S(2)}) copy-start(bf16[512,1024]{1,0:T(8,128)(2,1)} %get-tuple-element.268) | copy-start | bytes 3145732 | tf_op jit(solution)/shard_map/cond
  74.7 2.4 copy-start.4
  79.9 2.2 copy-start.9
  79.9 24.7 %copy-start.2 = (bf16[32,2048]{1,0:T(8,128)(2,1)S(1)}, bf16[32,2048]{1,0:T(8,128)(2,1)}, u32[]{:S(2)}) copy-start(bf16[32,2048]{1,0:T(8,128)(2,1)} %param.29) | copy-start | bytes 393220
  79.9 26.8 %copy-start.8 = (f32[2048]{0:T(1024)S(1)}, f32[2048]{0:T(1024)}, u32[]{:S(2)}) copy-start(f32[2048]{0:T(1024)} %param.30) | copy-start | bytes 24580
  81.2 122.7 %all-gather.8.cloned.1.call-start = ((), (), s32[]{:S(2)}) async-start(), calls=%async_computation.6 | async-start | bytes 1310720 | tf_op jit(solution)/shard_map/all_gather | solution.py:143
  123.2 53.6 %copy-start.12 = (bf16[1,2048,256]{2,1,0:T(8,128)(2,1)S(1)}, bf16[1,2048,256]{2,1,0:T(8,128)(2,1)}, u32[]{:S(2)}) copy-start(bf16[1,2048,256]{2,1,0:T(8,128)(2,1)} %param.33) | copy-start | bytes 3145732
  176.8 1.2 copy-start.13
  203.9 7.7 %copy-start.10 = (f32[128,2]{0,1:T(2,128)S(1)}, f32[128,2]{0,1:T(2,128)}, u32[]{:S(2)}) copy-start(f32[128,2]{0,1:T(2,128)} %param.32) | copy-start | bytes 3076
  207.0 19.9 %all-to-all-start.1 = ((bf16[8,64,512]{2,1,0:T(8,128)(2,1)}), bf16[8,64,512]{2,1,0:T(8,128)(2,1)S(1)}, u32[]{:S(2)}, u32[]{:S(2)}) async-start(bf16[8,64,512]{2,1,0:T(8,128)(2,1)} %bitcast.55), calls=%async_computation.2 | async-start | bytes 1048576 | tf_op jit(solution)/shard_map/all_to_all | solution.py:148
Sparse Core Ops, SparseCore 0:
  8.9 27.3 all-gather.3
  37.9 25.6 all-gather.5
  81.3 23.1 reduce-scatter.1
  179.5 24.3 all-gather.7
